TPU v7x, 32 devices: a whole 2x2x4 slice. The times are simulated.
32 devices in a mesh: ep: 8 (over z, x), tp: 4 (over y, core).
Axes of the slice: x: 2, y: 2, z: 4, core: 2. Of those that a mesh axis runs over, the one named last changes fastest.
Arguments:
- tokens: bfloat16 [128, 2048], P('ep'), may hold values from -120 to 120
- lengths: int32 [128], P('ep'), may hold values from 1 to 768, as said below
- cache_kv: bfloat16 [128, 768, 16, 128], P('ep', None, 'tp'), may hold values from -64 to 64
- cache_cum: float32 [128, 16, 768], P('ep', 'tp'), may hold values from -768 to 0, as said below
- norm_attn: float32 [2048], replicated, may hold values from 0.1 to 1.9
- w_query: bfloat16 [2048, 1024], P(None, 'tp'), may hold values from -0.125 to 0.125
- w_key: bfloat16 [2048, 1024], P(None, 'tp'), may hold values from -0.125 to 0.125
- w_value: bfloat16 [2048, 1024], P(None, 'tp'), may hold values from -0.125 to 0.125
- w_forget: bfloat16 [2048, 16], P(None, 'tp'), may hold values from -0.125 to 0.125
- b_forget: float32 [16], P('tp'), may hold values from -1 to 2
- w_output: bfloat16 [1024, 2048], P('tp'), may hold values from -0.1875 to 0.1875
- norm_ffn: float32 [2048], replicated, may hold values from 0.1 to 1.9
- shared_gate: bfloat16 [2048, 512], P(None, 'tp'), may hold values from -0.125 to 0.125
- shared_up: bfloat16 [2048, 512], P(None, 'tp'), may hold values from -0.125 to 0.125
- shared_down: bfloat16 [512, 2048], P('tp'), may hold values from -0.25 to 0.25
- expert_gate: bfloat16 [24, 2048, 512], P('ep', None, 'tp'), may hold values from -0.125 to 0.125
- expert_up: bfloat16 [24, 2048, 512], P('ep', None, 'tp'), may hold values from -0.125 to 0.125
- expert_down: bfloat16 [24, 512, 2048], P('ep', 'tp'), may hold values from -0.25 to 0.25
- route_ids: int32 [128, 6], P('ep'), may hold values from 0 to 23, all different within a row; in each aligned block of 16 rows (0 to 15, 16 to 31, ...) at most 8 rows name the same one
- route_weight: float32 [128, 6], P('ep'), may hold values from 0.1 to 0.8
Outputs:
- output: bfloat16 [128, 2048], P('ep', 'tp')
- new_kv: bfloat16 [128, 16, 128], P('ep', 'tp')
- new_cum: float32 [128, 16], P('ep', 'tp')
Inputs may be any that keep to these rules, and one draw needn't show every extreme that they name: `lengths`: every block of 16 sequences of one index of ep holds one with 768. `route_ids`: in the rows of one device (aligned blocks of 16 rows) no expert is named more than 8 times. `cache_cum`: Non-increasing along positions.
All inputs are finite; a program needn't handle non-finite values.
Results may differ from a plain program's by a relative error of at most 0.012.
Values may be sent and summed in bfloat16 or wider, within the bound.
A program may use at most 128 MiB of HBM per device.

v0:
```python
import jax
import jax.numpy as jnp
from jax import lax
from jax.sharding import PartitionSpec as P

HEAD_DIM = 64


epsilon = 1e-06


def rms_scale(row_block, gain):
    widened = row_block.astype(jnp.float32)
    return widened * lax.rsqrt(jnp.mean(widened * widened, axis=-1, keepdims=True) + epsilon) * gain


def shards(
    tokens,
    lengths,
    cache_kv,
    cache_cum,
    norm_attn,
    w_query,
    w_key,
    w_value,
    w_forget,
    b_forget,
    w_output,
    norm_ffn,
    shared_gate,
    shared_up,
    shared_down,
    expert_gate,
    expert_up,
    expert_down,
    route_ids,
    route_weight,
):
    ep_size = lax.axis_size("ep")
    tp_size = lax.axis_size("tp")
    tp_place = lax.axis_index("tp")
    seq_dev, model_width = tokens.shape
    width_part = model_width // tp_size
    heads_here = w_query.shape[1] // HEAD_DIM
    cache_len = cache_kv.shape[1]
    score_scale = HEAD_DIM ** (-0.5)
    normed = rms_scale(tokens, norm_attn).astype(jnp.bfloat16)
    queries = (
        jnp.dot(normed, w_query, preferred_element_type=jnp.float32)
        .astype(jnp.bfloat16)
        .reshape(seq_dev, heads_here, HEAD_DIM)
    )
    key_new = (
        jnp.dot(normed, w_key, preferred_element_type=jnp.float32)
        .astype(jnp.bfloat16)
        .reshape(seq_dev, heads_here, HEAD_DIM)
    )
    value_new = (
        jnp.dot(normed, w_value, preferred_element_type=jnp.float32)
        .astype(jnp.bfloat16)
        .reshape(seq_dev, heads_here, HEAD_DIM)
    )
    forget_log = jax.nn.log_sigmoid(
        jnp.dot(normed, w_forget, preferred_element_type=jnp.float32) + b_forget
    )
    last_index = jnp.broadcast_to((lengths - 1)[:, None, None], (seq_dev, heads_here, 1))
    cum_new = jnp.take_along_axis(cache_cum, last_index, axis=2)[:, :, 0] + forget_log
    past_scores = (
        jnp.einsum(
            "shd,slhd->shl",
            queries,
            cache_kv[:, :, :, :HEAD_DIM],
            preferred_element_type=jnp.float32,
        )
        * score_scale
    )
    past_scores = past_scores + cum_new[:, :, None] - cache_cum
    is_valid = jnp.arange(cache_len, dtype=jnp.int32)[None, None, :] < lengths[:, None, None]
    past_scores = jnp.where(is_valid, past_scores, -jnp.inf)
    own_score = (
        jnp.sum(queries.astype(jnp.float32) * key_new.astype(jnp.float32), axis=2) * score_scale
    )
    row_max = jnp.maximum(jnp.max(past_scores, axis=2), own_score)
    weights_past = jnp.exp(past_scores - row_max[:, :, None])
    weight_own = jnp.exp(own_score - row_max)
    weight_sum = jnp.sum(weights_past, axis=2) + weight_own
    probs_past = (weights_past / weight_sum[:, :, None]).astype(jnp.bfloat16)
    prob_own = (weight_own / weight_sum).astype(jnp.bfloat16)
    mixed = jnp.einsum(
        "shl,slhd->shd",
        probs_past,
        cache_kv[:, :, :, HEAD_DIM:],
        preferred_element_type=jnp.float32,
    )
    mixed = mixed + prob_own.astype(jnp.float32)[:, :, None] * value_new.astype(jnp.float32)
    attended = mixed.astype(jnp.bfloat16).reshape(seq_dev, heads_here * HEAD_DIM)
    partial_value = jnp.dot(attended, w_output, preferred_element_type=jnp.float32)
    summed = lax.psum(partial_value.astype(jnp.bfloat16), "tp").astype(jnp.float32)
    residual = (tokens.astype(jnp.float32) + summed).astype(jnp.bfloat16)
    ffn_in = rms_scale(residual, norm_ffn).astype(jnp.bfloat16)
    residual_part = lax.dynamic_slice_in_dim(residual, tp_place * width_part, width_part, 1)
    shared_hidden = (
        jax.nn.silu(jnp.dot(ffn_in, shared_gate, preferred_element_type=jnp.float32))
        * jnp.dot(ffn_in, shared_up, preferred_element_type=jnp.float32)
    ).astype(jnp.bfloat16)
    shared_part = jnp.dot(shared_hidden, shared_down, preferred_element_type=jnp.float32).astype(
        jnp.bfloat16
    )
    top_count = route_ids.shape[1]
    experts_here = expert_gate.shape[0]
    experts_all = experts_here * ep_size
    capacity = max(2, 2 * (seq_dev * top_count // experts_all))
    slot_count = experts_all * capacity
    route_flat = route_ids.reshape(-1)
    onehot = (route_flat[:, None] == jnp.arange(experts_all, dtype=jnp.int32)[None, :]).astype(
        jnp.int32
    )
    before = jnp.cumsum(onehot, axis=0) - onehot
    slot_rank = jnp.sum(before * onehot, axis=1)
    owner_index = route_flat // experts_here
    slot_local = route_flat % experts_here
    slot_index = ((slot_local * ep_size + owner_index) * capacity + slot_rank).reshape(
        seq_dev, top_count
    )
    slot_ids = jnp.arange(slot_count, dtype=jnp.int32)
    picker = jnp.sum(
        (slot_ids[:, None, None] == slot_index[None, :, :]).astype(jnp.bfloat16), axis=2
    )
    combine = jnp.sum(
        jnp.where(slot_ids[None, None, :] == slot_index[:, :, None], route_weight[:, :, None], 0.0),
        axis=1,
    )
    own_part = lax.dynamic_slice_in_dim(ffn_in, tp_place * width_part, width_part, 1)
    chosen = jnp.dot(picker, own_part, preferred_element_type=jnp.float32).astype(jnp.bfloat16)
    moved = lax.all_to_all(
        chosen.reshape(experts_here, ep_size, capacity, width_part),
        "ep",
        split_axis=1,
        concat_axis=1,
        tiled=True,
    )
    arrived = lax.all_gather(moved, "tp", axis=3, tiled=True)
    row_count = ep_size * capacity
    arrived = arrived.reshape(experts_here, row_count, model_width)
    gate_value = jnp.einsum(
        "erd,edf->erf", arrived, expert_gate, preferred_element_type=jnp.float32
    )
    up_value = jnp.einsum("erd,edf->erf", arrived, expert_up, preferred_element_type=jnp.float32)
    expert_hidden = (jax.nn.silu(gate_value) * up_value).astype(jnp.bfloat16)
    expert_part = jnp.einsum(
        "erf,efd->erd", expert_hidden, expert_down, preferred_element_type=jnp.float32
    ).astype(jnp.bfloat16)
    expert_pieces, shared_pieces = (
        lax.all_to_all(
            expert_part.reshape(experts_here, row_count, tp_size, width_part),
            "tp",
            split_axis=2,
            concat_axis=2,
            tiled=True,
        ),
        lax.all_to_all(
            shared_part.reshape(1, seq_dev, tp_size, width_part),
            "tp",
            split_axis=2,
            concat_axis=2,
            tiled=True,
        ),
    )
    expert_sum = jnp.sum(expert_pieces.astype(jnp.float32), axis=2).astype(jnp.bfloat16)
    shared_sum = jnp.sum(shared_pieces.astype(jnp.float32), axis=2)[0]
    returned = lax.all_to_all(
        expert_sum.reshape(experts_here, ep_size, capacity, width_part),
        "ep",
        split_axis=1,
        concat_axis=1,
        tiled=True,
    )
    routed = jnp.dot(
        combine,
        returned.reshape(slot_count, width_part).astype(jnp.float32),
        precision=lax.Precision.HIGHEST,
    )
    output = (residual_part.astype(jnp.float32) + shared_sum + routed).astype(jnp.bfloat16)
    new_kv = jnp.concatenate([key_new, value_new], axis=2)
    return (output, new_kv, cum_new)


def solution(mesh):
    in_specs = (
        P("ep", None),
        P("ep"),
        P("ep", None, "tp", None),
        P("ep", "tp", None),
        P(),
        P(None, "tp"),
        P(None, "tp"),
        P(None, "tp"),
        P(None, "tp"),
        P("tp"),
        P("tp", None),
        P(),
        P(None, "tp"),
        P(None, "tp"),
        P("tp", None),
        P("ep", None, "tp"),
        P("ep", None, "tp"),
        P("ep", "tp", None),
        P("ep", None),
        P("ep", None),
    )
    out_specs = (P("ep", "tp"), P("ep", "tp", None), P("ep", "tp"))
    return jax.shard_map(shards, mesh=mesh, in_specs=in_specs, out_specs=out_specs, check_vma=False)
```

profile of v0, /device:TPU:0, one launch (start us, length us, event | category | flops | bytes accessed | tf_op | source)
XLA Modules:
  0.0 160.5 jit_solution(2650859748003632178)
XLA Ops:
  7.2 0.8 broadcast_add_fusion
  8.0 0.7 broadcast_compare_fusion
  8.7 0.7 iota_compare_fusion.3
  9.4 1.0 fusion.23
  10.4 1.6 convolution_convert_fusion.6
  12.4 1.9 %gather_fusion = f32[64]{0:T(128)S(1)} fusion(f32[16,4,768]{2,1,0:T(4,128)} %param.23, s32[64]{0:T(128)S(1)} %reshape.286), kind=kCustom, calls=%fused_computation | custom fusion | bytes 1280 | tf_op jit(solution)/shard_map/jit(take_along_axis)/gather | solution.py:67
  14.5 1.1 fusion.52
  15.7 25.1 %fusion.69 = (bf16[16,768,4,64]{3,2,1,0:T(4,128)(2,1)}, bf16[16,768,4,64]{3,2,1,0:T(4,128)(2,1)}) fusion(bf16[16,768,4,128]{3,2,1,0:T(4,128)(2,1)} %param.22), kind=kLoop, calls=%fused_computation.112 | loop fusion | bytes 25165824 | tf_op jit(solution)/shard_map/slice | solution.py:72
  40.8 0.3 convolution_convert_fusion.5
  41.2 7.9 %fusion.2 = f32[16,4,1,768]{3,2,1,0:T(1,128)S(1)} fusion(bf16[16,4,64,1]{2,3,1,0:T(2,128)(2,1)S(1)} %reshape.299, bf16[16,768,4,64]{3,2,1,0:T(4,128)(2,1)} %get-tuple-element.7), kind=kOutput, calls=%fused_computation.3 | convolution fusion | flops 6291456 | bytes 6496256 | tf_op jit(solution)/shard_map/shd,slhd->shl/dot_general | solution.py:69
  49.9 0.3 convolution_convert_fusion.4
  50.3 6.4 %fusion = f32[16,4,1,64]{3,2,1,0:T(1,128)S(1)} fusion(bf16[16,768,4,64]{3,2,1,0:T(4,128)(2,1)} %get-tuple-element.8, bf16[16,4,768,1]{2,1,0,3:T(4,128)(2,1)S(1)} %fusion.32), kind=kOutput, calls=%fused_computation.1 | convolution fusion | flops 6291456 | bytes 6406144 | tf_op jit(solution)/shard_map/shl,slhd->shd/dot_general | solution.py:89
  56.9 0.9 convolution_convert_fusion.2
  58.7 33.5 %all-reduce.2.cloned.1.call-done = bf16[16,2048]{1,0:T(8,128)(2,1)} async-done(((bf16[16,2048]{1,0:T(8,128)(2,1)}), bf16[16,2048]{1,0:T(8,128)(2,1)}) %all-reduce.2.cloned.1.call-update) | async-done | bytes 65552 | tf_op jit(solution)/shard_map/psum | solution.py:98
  92.2 1.0 fusion.20
  93.5 13.1 %all_to_all.20 = bf16[3,8,8,512]{3,2,0,1:T(8,128)(2,1)S(1)} all-to-all(bf16[3,8,8,512]{3,2,0,1:T(8,128)(2,1)S(1)} %copy.73), channel_id=1, replica_groups=mesh['ep'=8,'tp'=4] {'ep'}, dimensions={1} | all-to-all | bytes 393216 | tf_op jit(solution)/shard_map/all_to_all | solution.py:135
  106.6 7.6 %all_gather.3 = bf16[3,8,8,2048]{3,2,0,1:T(8,128)(2,1)S(1)} all-gather(bf16[3,8,8,512]{3,2,0,1:T(8,128)(2,1)S(1)} %all_to_all.20), channel_id=1, replica_groups=mesh['ep'=8,'tp'=4] {'tp'}, dimensions={3}, use_global_device_ids=true | all-gather | bytes 983040 | tf_op jit(solution)/shard_map/all_gather | solution.py:142
  114.2 1.8 %fusion.10 = f32[3,64,128]{2,1,0:T(8,128)S(1)} fusion(bf16[3,2048,128]{2,1,0:T(8,128)(2,1)} %param.35, bf16[3,8,8,2048]{3,2,0,1:T(8,128)(2,1)S(1)} %all_gather.3), kind=kOutput, calls=%fused_computation.22 | convolution fusion | flops 100663296 | bytes 2457600 | tf_op jit(solution)/shard_map/erd,edf->erf/dot_general | solution.py:145
  116.0 2.0 %convolution_convert_fusion = bf16[3,64,2048]{2,1,0:T(8,128)(2,1)S(1)} fusion(bf16[3,128,2048]{2,1,0:T(8,128)(2,1)S(1)} %copy-done, bf16[3,2048,128]{2,1,0:T(8,128)(2,1)} %param.36, bf16[3,8,8,2048]{3,2,0,1:T(8,128)(2,1)S(1)} %all_gather.3, f32[3,64,128]{2,1,0:T(8,128)S(1)} %fusion.10), kind=kOutput, calls=%fused_computation.5 | convolution fusion | flops 201867264 | bytes 4816896 | tf_op jit(solution)/shard_map/erf,efd->erd/dot_general | solution.py:150
  118.1 1.0 copy.103
  119.0 3.5 %all-to-all-start.2 = ((bf16[3,64,4,512]{3,1,0,2:T(8,128)(2,1)}), bf16[3,64,4,512]{3,1,0,2:T(8,128)(2,1)S(1)}, u32[]{:S(2)}, u32[]{:S(2)}) async-start(bf16[3,64,4,512]{3,1,0,2:T(8,128)(2,1)} %bitcast.49), calls=%async_computation.2 | async-start | bytes 1572864 | tf_op jit(solution)/shard_map/all_to_all | solution.py:154
  122.5 1.2 fusion.70
  123.8 1.5 convolution_convert_fusion.1
  125.4 0.6 copy.66
  126.0 8.1 %all-to-all-done.2 = bf16[3,64,4,512]{3,1,0,2:T(8,128)(2,1)S(1)} async-done(((bf16[3,64,4,512]{3,1,0,2:T(8,128)(2,1)}), bf16[3,64,4,512]{3,1,0,2:T(8,128)(2,1)S(1)}, u32[]{:S(2)}, u32[]{:S(2)}) %all-to-all-start.2) | async-done | bytes 786464 | tf_op jit(solution)/shard_map/all_to_all | solution.py:154
  134.1 3.3 %all-to-all-start = ((bf16[1,16,4,512]{3,1,0,2:T(8,128)(2,1)}), bf16[1,16,4,512]{3,1,0,2:T(8,128)(2,1)S(1)}, u32[]{:S(2)}, u32[]{:S(2)}) async-start(bf16[1,16,4,512]{3,1,0,2:T(8,128)(2,1)} %copy.66), calls=%async_computation | async-start | bytes 131072 | tf_op jit(solution)/shard_map/all_to_all | solution.py:161
  137.6 0.7 copy.76
  138.3 3.2 %all-to-all-done = bf16[1,16,4,512]{3,1,0,2:T(8,128)(2,1)S(1)} async-done(((bf16[1,16,4,512]{3,1,0,2:T(8,128)(2,1)}), bf16[1,16,4,512]{3,1,0,2:T(8,128)(2,1)S(1)}, u32[]{:S(2)}, u32[]{:S(2)}) %all-to-all-start) | async-done | bytes 65568 | tf_op jit(solution)/shard_map/all_to_all | solution.py:161
  141.5 3.4 %all-to-all-start.3 = ((bf16[3,8,8,512]{3,2,0,1:T(8,128)(2,1)}), bf16[3,8,8,512]{3,2,0,1:T(8,128)(2,1)S(1)}, u32[]{:S(2)}, u32[]{:S(2)}) async-start(bf16[3,8,8,512]{3,2,0,1:T(8,128)(2,1)} %copy.76), calls=%async_computation.3 | async-start | bytes 393216 | tf_op jit(solution)/shard_map/all_to_all | solution.py:171
  144.9 0.7 pad_maximum_fusion
  145.7 7.2 %all-to-all-done.3 = bf16[3,8,8,512]{3,2,0,1:T(8,128)(2,1)S(1)} async-done(((bf16[3,8,8,512]{3,2,0,1:T(8,128)(2,1)}), bf16[3,8,8,512]{3,2,0,1:T(8,128)(2,1)S(1)}, u32[]{:S(2)}, u32[]{:S(2)}) %all-to-all-start.3) | async-done | bytes 196640 | tf_op jit(solution)/shard_map/all_to_all | solution.py:171
  152.9 0.8 fusion.5
  (65 shorter events, 3.4 us)
Async XLA Ops:
  7.2 108.9 %copy-start = (bf16[3,128,2048]{2,1,0:T(8,128)(2,1)S(1)}, bf16[3,128,2048]{2,1,0:T(8,128)(2,1)}, u32[]{:S(2)}) copy-start(bf16[3,128,2048]{2,1,0:T(8,128)(2,1)} %param.37) | copy-start | bytes 4718596
  7.2 85.0 %all-reduce.2.cloned.1.call-start = ((), (), s32[]{:S(2)}) async-start(), calls=%async_computation.4 | async-start | bytes 131072 | tf_op jit(solution)/shard_map/psum | solution.py:98
  15.6 25.2 %copy-start.10 = (f32[16,4]{0,1:T(4,128)}, f32[16,4]{0,1:T(4,128)S(1)}, u32[]{:S(2)}) copy-start(f32[16,4]{0,1:T(4,128)S(1)} %fusion.52) | copy-start | bytes 772
  15.6 25.1 %copy-start.2 = (bf16[16,2048]{1,0:T(8,128)(2,1)S(1)}, bf16[16,2048]{1,0:T(8,128)(2,1)}, u32[]{:S(2)}) copy-start(bf16[16,2048]{1,0:T(8,128)(2,1)} %param.20) | copy-start | bytes 196612
  15.7 25.1 %copy-start.3 = (bf16[2048,256]{1,0:T(8,128)(2,1)S(1)}, bf16[2048,256]{1,0:T(8,128)(2,1)}, u32[]{:S(2)}) copy-start(bf16[2048,256]{1,0:T(8,128)(2,1)} %param.26) | copy-start | bytes 3145732
  15.7 25.1 %copy-start.6 = (f32[2048]{0:T(1024)S(1)}, f32[2048]{0:T(1024)}, u32[]{:S(2)}) copy-start(f32[2048]{0:T(1024)} %param.24) | copy-start | bytes 24580
  40.8 8.4 %copy-start.1 = (f32[16,4,768]{2,1,0:T(4,128)S(1)}, f32[16,4,768]{2,1,0:T(4,128)}, u32[]{:S(2)}) copy-start(f32[16,4,768]{2,1,0:T(4,128)} %param.23) | copy-start | bytes 589828
  40.8 9.1 %copy-start.4 = (bf16[2048,256]{1,0:T(8,128)(2,1)S(1)}, bf16[2048,256]{1,0:T(8,128)(2,1)}, u32[]{:S(2)}) copy-start(bf16[2048,256]{1,0:T(8,128)(2,1)} %param.27) | copy-start | bytes 3145732
  50.2 6.7 %copy-start.5 = (bf16[256,2048]{1,0:T(8,128)(2,1)S(1)}, bf16[256,2048]{1,0:T(8,128)(2,1)}, u32[]{:S(2)}) copy-start(bf16[256,2048]{1,0:T(8,128)(2,1)} %param.30) | copy-start | bytes 3145732
  50.3 7.5 %copy-start.8 = (s32[16,6]{0,1:T(8,128)S(1)}, s32[16,6]{0,1:T(8,128)}, u32[]{:S(2)}) copy-start(s32[16,6]{0,1:T(8,128)} %param.38) | copy-start | bytes 1156
  50.3 42.9 %copy-start.7 = (f32[2048]{0:T(1024)S(1)}, f32[2048]{0:T(1024)}, u32[]{:S(2)}) copy-start(f32[2048]{0:T(1024)} %param.31) | copy-start | bytes 24580
  56.7 88.9 %copy-start.9 = (f32[16,6]{0,1:T(8,128)S(1)}, f32[16,6]{0,1:T(8,128)}, u32[]{:S(2)}) copy-start(f32[16,6]{0,1:T(8,128)} %param.39) | copy-start | bytes 1156
  119.0 15.1 %all-to-all-start.2 = ((bf16[3,64,4,512]{3,1,0,2:T(8,128)(2,1)}), bf16[3,64,4,512]{3,1,0,2:T(8,128)(2,1)S(1)}, u32[]{:S(2)}, u32[]{:S(2)}) async-start(bf16[3,64,4,512]{3,1,0,2:T(8,128)(2,1)} %bitcast.49), calls=%async_computation.2 | async-start | bytes 1572864 | tf_op jit(solution)/shard_map/all_to_all | solution.py:154
  134.1 7.4 %all-to-all-start = ((bf16[1,16,4,512]{3,1,0,2:T(8,128)(2,1)}), bf16[1,16,4,512]{3,1,0,2:T(8,128)(2,1)S(1)}, u32[]{:S(2)}, u32[]{:S(2)}) async-start(bf16[1,16,4,512]{3,1,0,2:T(8,128)(2,1)} %copy.66), calls=%async_computation | async-start | bytes 131072 | tf_op jit(solution)/shard_map/all_to_all | solution.py:161
  141.5 11.4 %all-to-all-start.3 = ((bf16[3,8,8,512]{3,2,0,1:T(8,128)(2,1)}), bf16[3,8,8,512]{3,2,0,1:T(8,128)(2,1)S(1)}, u32[]{:S(2)}, u32[]{:S(2)}) async-start(bf16[3,8,8,512]{3,2,0,1:T(8,128)(2,1)} %copy.76), calls=%async_computation.3 | async-start | bytes 393216 | tf_op jit(solution)/shard_map/all_to_all | solution.py:171
Sparse Core Ops, SparseCore 0:
  57.9 34.2 all-reduce.1
where the time goes:
time: 162 us; the launch traced here: 161 us
  waiting for transfers between devices  52.1 us (32%)
  local copies, waits for them, and re-layouts  30.6 us (19%)
  matrix products  26.1 us (16%)
  blocking collectives  20.7 us (13%)
  between operations  14.4 us (9%)
  starting transfers between devices  10.2 us (6%)
  other arithmetic  6.52 us (4%)
    psum x1, waiting for transfers between devices, shards(): lax.psum(partial_value.astype(jnp.bfloat16), 'tp').astype(jnp.float32)  33.5 us
    slice x1, local copies, waits for them, and re-layouts, shards(): cache_kv[:, :, :, :HEAD_DIM]  25.1 us
    all_to_all x1, blocking collectives, shards(): lax.all_to_all(chosen.reshape(experts_here, ep_size, capacity, width_part...  13.1 us
    all_to_all x1, waiting for transfers between devices, shards(): lax.all_to_all(expert_part.reshape(experts_here, row_count, tp_size, widt...  8.13 us
    dot_general x1, matrix products, shards(): jnp.einsum('shd,slhd->shl', queries, cache_kv[:, :, :, :HEAD_DIM], prefer...  7.93 us
    all_gather x1, blocking collectives, shards(): arrived = lax.all_gather(moved, 'tp', axis=3, tiled=True)  7.59 us
    all_to_all x1, waiting for transfers between devices, shards(): lax.all_to_all(expert_sum.reshape(experts_here, ep_size, capacity, width_...  7.17 us
    dot_general x1, matrix products, shards(): jnp.einsum('shl,slhd->shd', probs_past, cache_kv[:, :, :, HEAD_DIM:], pre...  6.38 us
  transfers between devices with their start and end apart: 4, of which 4 were waited for; matrix products, arithmetic and copies ran while one was open for 4% of the time, Pallas kernels for 0%

commit v1 on v0

--- a/solution.py
+++ b/solution.py
@@ -1,20 +1,570 @@
+import functools
+
 import jax
 import jax.numpy as jnp
 from jax import lax
+from jax.experimental import pallas as pl
+from jax.experimental.pallas import tpu as pltpu
 from jax.sharding import PartitionSpec as P
 
 HEAD_DIM = 64
-
-
+LANES = 128
 epsilon = 1e-06
+MESH = pl.DeviceIdType.MESH
+F32 = jnp.float32
+BF16 = jnp.bfloat16
 
 
 def rms_scale(row_block, gain):
-    widened = row_block.astype(jnp.float32)
+    widened = row_block.astype(F32)
     return widened * lax.rsqrt(jnp.mean(widened * widened, axis=-1, keepdims=True) + epsilon) * gain
 
 
+def attention_kernel(
+    group,
+    lengths_ref,
+    tokens_ref,
+    cum_ref,
+    gain_ref,
+    wf_ref,
+    bf_ref,
+    wq_hbm,
+    wk_hbm,
+    wv_hbm,
+    wo_hbm,
+    kv_hbm,
+    partial_ref,
+    new_kv_ref,
+    new_cum_ref,
+    wq,
+    wk,
+    wv,
+    wo,
+    kv,
+    q_pad,
+    fresh,
+    forget,
+    cum_new,
+    mixed_all,
+    w_sem,
+    kv_sem,
+):
+    seqs = tokens_ref.shape[0]
+    heads = new_kv_ref.shape[1]
+    columns = kv.shape[1]
+    rows = q_pad.shape[1]
+    scale = HEAD_DIM ** (-0.5)
+    w_copies = [
+        pltpu.make_async_copy(src, dst, w_sem.at[i])
+        for i, (src, dst) in enumerate(((wq_hbm, wq), (wk_hbm, wk), (wv_hbm, wv), (wo_hbm, wo)))
+    ]
+
+    def kv_copy(s):
+        return pltpu.make_async_copy(kv_hbm.at[s], kv.at[s], kv_sem.at[s])
+
+    for copy in w_copies[:3]:
+        copy.start()
+    for s in range(seqs):
+        kv_copy(s).start()
+    w_copies[3].start()
+
+    normed = rms_scale(tokens_ref[...], gain_ref[...]).astype(BF16)
+    forget_log = jax.nn.log_sigmoid(
+        lax.dot_general(
+            normed, wf_ref[...], (((1,), (1,)), ((), ())), preferred_element_type=F32
+        )
+        + bf_ref[...]
+    )
+    q_pad[...] = jnp.zeros_like(q_pad)
+    fresh[...] = jnp.zeros_like(fresh)
+    forget[...] = jnp.zeros_like(forget)
+    lane = lax.broadcasted_iota(jnp.int32, (seqs, LANES), 1)
+    low = lane < HEAD_DIM
+    for copy in w_copies[:3]:
+        copy.wait()
+    queries, keys, values = (
+        jnp.dot(normed, w[...], preferred_element_type=F32).astype(BF16).astype(F32)
+        for w in (wq, wk, wv)
+    )
+    for h in range(heads):
+        pair = slice((h // 2) * LANES, (h // 2 + 1) * LANES)
+        q_h, k_h, v_h = queries[:, pair], keys[:, pair], values[:, pair]
+        if h % 2 == 0:
+            v_h = pltpu.roll(v_h, HEAD_DIM, 1)
+        else:
+            q_h = pltpu.roll(q_h, HEAD_DIM, 1)
+            k_h = pltpu.roll(k_h, HEAD_DIM, 1)
+        q_pad[:, h, :] = jnp.where(low, q_h, 0.0)
+        fresh[:, h, :] = jnp.where(low, k_h, v_h)
+        forget[:, h, :] = jnp.broadcast_to(forget_log[:, h : h + 1], (seqs, LANES))
+    new_kv_ref[...] = fresh[:, :heads, :].astype(BF16)
+
+    column = lax.broadcasted_iota(jnp.int32, (rows, columns), 1)
+    own_head = lax.rem(column, heads) == lax.broadcasted_iota(jnp.int32, (rows, columns), 0)
+
+    def attend(s):
+        kv_copy(s).wait()
+        length = lengths_ref[s]
+        rows_kv = kv[s]
+        q = q_pad[s]
+        new = fresh[s]
+        cum = cum_ref[s]
+        scores = lax.dot_general(
+            q.astype(BF16), rows_kv, (((1,), (1,)), ((), ())), preferred_element_type=F32
+        )
+        last = own_head & (column >= (length - 1) * heads) & (column < length * heads)
+        cum_here = jnp.sum(jnp.where(last, cum, 0.0), axis=1, keepdims=True) + forget[s][:, :1]
+        cum_new[s] = jnp.broadcast_to(cum_here, (rows, LANES))
+        valid = own_head & (column < length * heads)
+        scores = jnp.where(valid, scores * scale + cum_here - cum, -jnp.inf)
+        own = jnp.sum(q * new, axis=1, keepdims=True) * scale
+        top = jnp.maximum(jnp.max(scores, axis=1, keepdims=True), own)
+        terms = jnp.exp(scores - top)
+        own_term = jnp.exp(own - top)
+        total = jnp.sum(terms, axis=1, keepdims=True) + own_term
+        inverse = 1.0 / total
+        probs = (terms * inverse).astype(BF16)
+        prob_own = (own_term * inverse).astype(BF16).astype(F32)
+        mixed = jnp.dot(probs, rows_kv, preferred_element_type=F32) + prob_own * new
+        mixed_all[s] = mixed.astype(BF16).astype(F32)
+
+    def attend_group(i, carry):
+        for j in range(group):
+            attend(i * group + j)
+        return carry
+
+    lax.fori_loop(0, seqs // group, attend_group, 0)
+
+    attended = jnp.concatenate(
+        [
+            jnp.where(low, pltpu.roll(mixed_all[:, h, :], HEAD_DIM, 1), mixed_all[:, h + 1, :])
+            for h in range(0, heads, 2)
+        ],
+        axis=1,
+    ).astype(BF16)
+    gathered = jnp.zeros((seqs, LANES), F32)
+    for h in range(heads):
+        gathered = jnp.where(lane == h, cum_new[:, h, :], gathered)
+    new_cum_ref[...] = gathered[:, :heads]
+    w_copies[3].wait()
+    partial_ref[...] = jnp.dot(attended, wo[...], preferred_element_type=F32).astype(BF16)
+
+
+def expert_kernel(
+    ep_size,
+    tp_size,
+    partial_ref,
+    tokens_ref,
+    gain_ref,
+    ids_ref,
+    weight_ref,
+    sg_hbm,
+    su_hbm,
+    sd_hbm,
+    eg_hbm,
+    eu_hbm,
+    ed_hbm,
+    out_ref,
+    swgu,
+    swd,
+    wgu,
+    wd,
+    sums,
+    blocks,
+    parts,
+    from_core,
+    to_y,
+    from_y,
+    to_x,
+    from_x,
+    to_z,
+    from_z,
+    w_sem,
+    ar_send,
+    ar_recv,
+    ag_recv,
+    z_send,
+    x_send,
+    d_send,
+    core_send,
+    core_recv,
+    yx_send,
+    yx_recv,
+    rz_send,
+    rz_recv,
+):
+    seqs, width = tokens_ref.shape
+    quarter = width // tp_size
+    half = width // 2
+    experts = eg_hbm.shape[0]
+    hidden = eg_hbm.shape[2]
+    nx = 2
+    nz = ep_size // nx
+    e = lax.axis_index("ep")
+    t = lax.axis_index("tp")
+    z, x = e // nx, e % nx
+    y, c = t // 2, t % 2
+    x_peer = z * nx + (1 - x)
+    core_peer = y * 2 + (1 - c)
+    y_peer = (1 - y) * 2 + c
+
+    def slot_of(z_at, x_at):
+        return x_at * nz + z_at
+
+    def z_at(d):
+        return lax.rem(z + d, nz)
+
+    weight_copies = []
+    for i in range(experts):
+        weight_copies.append((eg_hbm.at[i], wgu.at[i, :, pl.ds(0, hidden)]))
+        weight_copies.append((eu_hbm.at[i], wgu.at[i, :, pl.ds(hidden, hidden)]))
+        weight_copies.append((ed_hbm.at[i], wd.at[pl.ds(i * hidden, hidden), :]))
+    weight_copies.append((sg_hbm, swgu.at[:, pl.ds(0, hidden)]))
+    weight_copies.append((su_hbm, swgu.at[:, pl.ds(hidden, hidden)]))
+    weight_copies.append((sd_hbm, swd))
+    weight_copies = [
+        pltpu.make_async_copy(s, d, w_sem.at[i]) for i, (s, d) in enumerate(weight_copies)
+    ]
+    shared_copies, expert_copies = weight_copies[-3:], weight_copies[:-3]
+
+    barrier = pltpu.get_barrier_semaphore()
+    peers = [(e, lax.rem(t + k, tp_size)) for k in range(1, tp_size)]
+    peers += [(z_at(d) * nx + x, t) for d in range(1, nz)]
+    peers += [(x_peer, t)]
+    for peer in peers:
+        pl.semaphore_signal(barrier, inc=1, device_id=peer, device_id_type=MESH)
+    for copy in shared_copies + expert_copies:
+        copy.start()
+    pl.semaphore_wait(barrier, len(peers))
+
+    def remote(src, dst, send, recv, peer):
+        return pltpu.make_async_remote_copy(
+            src_ref=src,
+            dst_ref=dst,
+            send_sem=send,
+            recv_sem=recv,
+            device_id=peer,
+            device_id_type=MESH,
+        )
+
+    ar_copies = [
+        remote(
+            partial_ref,
+            sums.at[k - 1],
+            ar_send.at[k - 1],
+            ar_recv.at[k - 1],
+            (e, lax.rem(t + k, tp_size)),
+        )
+        for k in range(1, tp_size)
+    ]
+    for copy in ar_copies:
+        copy.start()
+    pad = blocks.shape[3] - half
+    expert_lane = lax.broadcasted_iota(jnp.int32, (seqs, pad), 1)
+    dense = jnp.zeros((seqs, pad), F32)
+    for k in range(ids_ref.shape[1]):
+        dense += jnp.where(ids_ref[:, k : k + 1] == expert_lane, weight_ref[:, k : k + 1], 0.0)
+    total = partial_ref[...].astype(F32)
+    for k, copy in enumerate(ar_copies):
+        copy.wait()
+        total += sums[k].astype(F32)
+    residual = (tokens_ref[...].astype(F32) + total).astype(BF16)
+    ffn_in = rms_scale(residual, gain_ref[...]).astype(BF16)
+    sums[0] = residual
+    mine = slot_of(z, x)
+    for h in range(2):
+        blocks[mine, h, :, :half] = ffn_in[:, h * half : (h + 1) * half]
+        blocks[mine, h, :, half:] = dense.astype(BF16)
+
+    def z_copy(d, source):
+        return remote(
+            blocks.at[source, c],
+            blocks.at[source, c],
+            z_send.at[d - 1],
+            ag_recv.at[source, c],
+            (z_at(d) * nx + x, t),
+        )
+
+    def x_copy(source):
+        return remote(
+            blocks.at[source, c],
+            blocks.at[source, c],
+            x_send.at[source],
+            ag_recv.at[source, c],
+            (x_peer, t),
+        )
+
+    def d_copy(source):
+        return remote(
+            blocks.at[source, c],
+            blocks.at[source, c],
+            d_send.at[source],
+            ag_recv.at[source, c],
+            (e, core_peer),
+        )
+
+    def arrived(source, part):
+        remote(
+            blocks.at[source, part],
+            blocks.at[source, part],
+            d_send.at[source],
+            ag_recv.at[source, part],
+            (e, core_peer),
+        ).wait_recv()
+
+    x_copy(mine).start()
+    for d in range(1, nz):
+        z_copy(d, mine).start()
+
+    for copy in shared_copies:
+        copy.wait()
+    both = jnp.dot(ffn_in, swgu[...], preferred_element_type=F32)
+    shared_hidden = (jax.nn.silu(both[:, :hidden]) * both[:, hidden:]).astype(BF16)
+
+    others_x = [slot_of(z, 1 - x)]
+    arrived(others_x[0], c)
+    d_copy(others_x[0]).start()
+    others_z = []
+    for d in range(1, nz):
+        source = slot_of(lax.rem(z + nz - d, nz), x)
+        others_z.append(source)
+        arrived(source, c)
+        x_copy(source).start()
+        d_copy(source).start()
+    for d in range(1, nz):
+        source = slot_of(lax.rem(z + nz - d, nz), 1 - x)
+        others_x.append(source)
+        arrived(source, c)
+        d_copy(source).start()
+    for copy in expert_copies:
+        copy.wait()
+    for source in others_x + others_z:
+        arrived(source, 1 - c)
+
+    token_count = ep_size * seqs
+    first = blocks[:, 0, :, :half].reshape(token_count, half)
+    second = blocks[:, 1, :, :half].reshape(token_count, half)
+    gathered = blocks[:, 0, :, half:].reshape(token_count, pad).astype(F32)
+    pad_lane = lax.broadcasted_iota(jnp.int32, (token_count, pad), 1)
+    pieces = []
+    for i in range(experts):
+        both = jnp.dot(first, wgu[i, :half, :], preferred_element_type=F32)
+        both += jnp.dot(second, wgu[i, half:, :], preferred_element_type=F32)
+        scale = jnp.sum(
+            jnp.where(pad_lane == e * experts + i, gathered, 0.0), axis=1, keepdims=True
+        )
+        pieces.append((jax.nn.silu(both[:, :hidden]) * both[:, hidden:] * scale).astype(BF16))
+    expert_hidden = jnp.concatenate(pieces, axis=1)
+
+    own_rows = pl.ds(pl.multiple_of(mine * seqs, seqs), seqs)
+
+    def column_block(index):
+        return pl.ds(pl.multiple_of(index * quarter, LANES), quarter)
+
+    core_copies = []
+    for k in range(2):
+        cols = column_block(2 * k + 1 - c)
+        value = jnp.dot(expert_hidden, wd[:, cols], preferred_element_type=F32)
+        parts[k] = value.astype(BF16)
+        shared = jnp.dot(shared_hidden, swd[:, cols], preferred_element_type=F32)
+        parts[k, own_rows, :] = (parts[k, own_rows, :].astype(F32) + shared).astype(BF16)
+        copy = remote(
+            parts.at[k], from_core.at[k], core_send.at[k], core_recv.at[k], (e, core_peer)
+        )
+        copy.start()
+        core_copies.append(copy)
+
+    def own_part(k, y_index):
+        cols = column_block(2 * y_index + c)
+        to_ref = to_y if k == 0 else to_x
+        shared = jnp.dot(shared_hidden, swd[:, cols], preferred_element_type=F32)
+        to_ref[...] = jnp.dot(expert_hidden, wd[:, cols], preferred_element_type=F32)
+        to_ref[own_rows, :] = to_ref[own_rows, :] + shared
+
+    own_part(0, 1 - y)
+    own_part(1, y)
+    for copy in core_copies:
+        copy.wait()
+    parts[0] = (to_y[...] + from_core[1 - y].astype(F32)).astype(BF16)
+    y_copy = remote(parts.at[0], from_y, yx_send.at[0], yx_recv.at[0], (e, y_peer))
+    y_copy.start()
+    to_x[...] = to_x[...] + from_core[y].astype(F32)
+    y_copy.wait()
+    half_rows = nz * seqs
+    there = pl.ds(pl.multiple_of((1 - x) * half_rows, seqs), half_rows)
+    here = pl.ds(pl.multiple_of(x * half_rows, seqs), half_rows)
+    parts[1, :half_rows, :] = (to_x[there, :] + from_y[there, :].astype(F32)).astype(BF16)
+    x_out = remote(
+        parts.at[1, pl.ds(0, half_rows)], from_x, yx_send.at[1], yx_recv.at[1], (x_peer, t)
+    )
+    x_out.start()
+    to_y[:half_rows, :] = to_x[here, :] + from_y[here, :].astype(F32)
+    x_out.wait()
+    to_y[:half_rows, :] = to_y[:half_rows, :] + from_x[...].astype(F32)
+    to_z[...] = to_y[:half_rows, :].astype(BF16)
+    rz_copies = []
+    for d in range(1, nz):
+        rows = pl.ds(pl.multiple_of(z_at(d) * seqs, seqs), seqs)
+        rz_copies.append(
+            remote(
+                to_z.at[rows],
+                from_z.at[d - 1],
+                rz_send.at[d - 1],
+                rz_recv.at[d - 1],
+                (z_at(d) * nx + x, t),
+            )
+        )
+        rz_copies[-1].start()
+    my_columns = pl.ds(pl.multiple_of(t * quarter, LANES), quarter)
+    result = sums[0, :, my_columns].astype(F32)
+    result += to_y[pl.ds(pl.multiple_of(z * seqs, seqs), seqs), :]
+    for d, copy in enumerate(rz_copies):
+        copy.wait()
+        result += from_z[d].astype(F32)
+    out_ref[...] = result.astype(BF16)
+
+    for copy in [x_copy(mine)] + [z_copy(d, mine) for d in range(1, nz)]:
+        copy.wait_send()
+    for source in others_z:
+        x_copy(source).wait_send()
+    for source in others_x + others_z:
+        d_copy(source).wait_send()
+
+
 def shards(
+    tokens,
+    lengths,
+    cache_kv,
+    cache_cum,
+    norm_attn,
+    w_query,
+    w_key,
+    w_value,
+    w_forget,
+    b_forget,
+    w_output,
+    norm_ffn,
+    shared_gate,
+    shared_up,
+    shared_down,
+    expert_gate,
+    expert_up,
+    expert_down,
+    route_ids,
+    route_weight,
+):
+    ep_size = lax.axis_size("ep")
+    tp_size = lax.axis_size("tp")
+    seqs, width = tokens.shape
+    cache_len, heads = cache_kv.shape[1], cache_kv.shape[2]
+    projected = w_query.shape[1]
+    columns = cache_len * heads
+    head_rows = -(-heads // 8) * 8
+    vmem = pl.BlockSpec(memory_space=pltpu.VMEM)
+    smem = pl.BlockSpec(memory_space=pltpu.SMEM)
+    anywhere = pl.BlockSpec(memory_space=pl.ANY)
+    kv_rows = cache_kv.reshape(seqs, columns, 2 * HEAD_DIM)
+    cum_rows = cache_cum.transpose(0, 2, 1).reshape(seqs, 1, columns)
+    per_head = pltpu.VMEM((seqs, head_rows, LANES), F32)
+    partial, new_kv, cum_new = pl.pallas_call(
+        functools.partial(attention_kernel, 4),
+        out_shape=(
+            jax.ShapeDtypeStruct((seqs, width), BF16),
+            jax.ShapeDtypeStruct((seqs, heads, 2 * HEAD_DIM), BF16),
+            jax.ShapeDtypeStruct((seqs, heads), F32),
+        ),
+        in_specs=[smem] + [vmem] * 5 + [anywhere] * 5,
+        out_specs=(vmem, vmem, vmem),
+        scratch_shapes=[
+            pltpu.VMEM((width, projected), BF16),
+            pltpu.VMEM((width, projected), BF16),
+            pltpu.VMEM((width, projected), BF16),
+            pltpu.VMEM((projected, width), BF16),
+            pltpu.VMEM((seqs, columns, 2 * HEAD_DIM), BF16),
+            per_head,
+            per_head,
+            per_head,
+            per_head,
+            per_head,
+            pltpu.SemaphoreType.DMA((4,)),
+            pltpu.SemaphoreType.DMA((seqs,)),
+        ],
+        compiler_params=pltpu.CompilerParams(vmem_limit_bytes=60 * 2**20),
+        name="attention",
+    )(
+        lengths,
+        tokens,
+        cum_rows,
+        norm_attn.reshape(1, width),
+        w_forget.T,
+        b_forget.reshape(1, heads),
+        w_query,
+        w_key,
+        w_value,
+        w_output,
+        kv_rows,
+    )
+    experts, _, hidden = expert_gate.shape
+    quarter = width // tp_size
+    token_count = ep_size * seqs
+    nz = ep_size // 2
+    pad = -(-experts * ep_size // LANES) * LANES
+    dma = pltpu.SemaphoreType.DMA
+    output = pl.pallas_call(
+        functools.partial(expert_kernel, ep_size, tp_size),
+        out_shape=jax.ShapeDtypeStruct((seqs, quarter), BF16),
+        in_specs=[vmem] * 5 + [anywhere] * 6,
+        out_specs=vmem,
+        scratch_shapes=[
+            pltpu.VMEM((width, 2 * hidden), BF16),
+            pltpu.VMEM((hidden, width), BF16),
+            pltpu.VMEM((experts, width, 2 * hidden), BF16),
+            pltpu.VMEM((experts * hidden, width), BF16),
+            pltpu.VMEM((tp_size - 1, seqs, width), BF16),
+            pltpu.VMEM((ep_size, 2, seqs, width // 2 + pad), BF16),
+            pltpu.VMEM((2, token_count, quarter), BF16),
+            pltpu.VMEM((2, token_count, quarter), BF16),
+            pltpu.VMEM((token_count, quarter), F32),
+            pltpu.VMEM((token_count, quarter), BF16),
+            pltpu.VMEM((token_count, quarter), F32),
+            pltpu.VMEM((nz * seqs, quarter), BF16),
+            pltpu.VMEM((nz * seqs, quarter), BF16),
+            pltpu.VMEM((nz - 1, seqs, quarter), BF16),
+            dma((3 * experts + 3,)),
+            dma((tp_size - 1,)),
+            dma((tp_size - 1,)),
+            dma((ep_size, 2)),
+            dma((nz - 1,)),
+            dma((ep_size,)),
+            dma((ep_size,)),
+            dma((2,)),
+            dma((2,)),
+            dma((2,)),
+            dma((2,)),
+            dma((nz - 1,)),
+            dma((nz - 1,)),
+        ],
+        compiler_params=pltpu.CompilerParams(
+            collective_id=0, has_side_effects=True, vmem_limit_bytes=60 * 2**20
+        ),
+        name="experts",
+    )(
+        partial,
+        tokens,
+        norm_ffn.reshape(1, width),
+        route_ids,
+        route_weight,
+        shared_gate,
+        shared_up,
+        shared_down,
+        expert_gate,
+        expert_up,
+        expert_down,
+    )
+    return (output, new_kv, cum_new)
+
+
+def shards_general(
     tokens,
     lengths,
     cache_kv,
@@ -209,4 +759,6 @@
         P("ep", None),
     )
     out_specs = (P("ep", "tp"), P("ep", "tp", None), P("ep", "tp"))
-    return jax.shard_map(shards, mesh=mesh, in_specs=in_specs, out_specs=out_specs, check_vma=False)
+    fused = mesh.shape["tp"] == 4 and mesh.shape["ep"] % 2 == 0 and mesh.shape["ep"] > 2
+    body = shards if fused else shards_general
+    return jax.shard_map(body, mesh=mesh, in_specs=in_specs, out_specs=out_specs, check_vma=False)

time: 162 us -> 60.8 us (0.38)
  Pallas kernels: 0 us -> 53.9 us
  waiting for transfers between devices: 52.1 us -> 0 us
  matrix products: 26.1 us -> 0 us
  local copies, waits for them, and re-layouts: 30.6 us -> 6.01 us
  blocking collectives: 20.7 us -> 0 us
  between operations: 14.4 us -> 0.67 us
  starting transfers between devices: 10.2 us -> 0 us
  other arithmetic: 6.52 us -> 0 us
    pallas_call x0 -> x2, Pallas kernels: none -> 53.9 us  [the longest x1 34.4 us: shards(): pl.pallas_call(functools.partial(expert_kernel, ep_size, tp_size), out_sh...]
    psum x1 -> x0, waiting for transfers between devices: 33.5 us -> none  [shards(): lax.psum(partial_value.astype(jnp.bfloat16), 'tp').astype(jnp.float32)]
    dot_general x13 -> x0, matrix products: 26.1 us -> none  [the longest x1 7.93 us: shards(): jnp.einsum('shd,slhd->shl', queries, cache_kv[:, :, :, :HEAD_DIM], prefer...]
    slice x1 -> x0, local copies, waits for them, and re-layouts: 25.1 us -> none  [shards(): cache_kv[:, :, :, :HEAD_DIM]]
    all_to_all x3 -> x0, waiting for transfers between devices: 18.5 us -> none  [the longest x1 8.13 us: shards(): lax.all_to_all(expert_part.reshape(experts_here, row_count, tp_size, widt...]
    all_to_all x1 -> x0, blocking collectives: 13.1 us -> none  [shards(): lax.all_to_all(chosen.reshape(experts_here, ep_size, capacity, width_part...]
    all_to_all x3 -> x0, starting transfers between devices: 10.2 us -> none  [the longest x1 3.49 us: shards(): lax.all_to_all(expert_part.reshape(experts_here, row_count, tp_size, widt...]
    all_gather x1 -> x0, blocking collectives: 7.59 us -> none  [shards(): arrived = lax.all_gather(moved, 'tp', axis=3, tiled=True)]
  transfers between devices with their start and end apart: 4 -> 0, of which waited for: 4 -> 0; matrix products, arithmetic and copies ran while one was open for 4% -> 0% of each run, Pallas kernels for 0% -> 0%
where the time goes in v1:
time: 60.8 us; the launch traced here: 60.5 us
  Pallas kernels  53.9 us (89%)
  local copies, waits for them, and re-layouts  6.01 us (10%)
  between operations  0.67 us (1%)
    pallas_call x1, Pallas kernels, shards(): pl.pallas_call(functools.partial(expert_kernel, ep_size, tp_size), out_sh...  34.4 us
    pallas_call x1, Pallas kernels, shards(): pl.pallas_call(functools.partial(attention_kernel, 4), out_shape=(jax.Sha...  19.5 us
    unnamed x10, local copies, waits for them, and re-layouts  3.34 us
    transpose x1, local copies, waits for them, and re-layouts, shards(): cum_rows = cache_cum.transpose(0, 2, 1).reshape(seqs, 1, columns)  1.55 us

profile of v1, /device:TPU:0, one launch (start us, length us, event | category | flops | bytes accessed | tf_op | source)
XLA Modules:
  0.0 60.5 jit_solution(4715395778807957037)
XLA Ops:
  0.6 1.6 %copy.27 = f32[16,768,4]{0,2,1:T(4,128)S(1)} copy(f32[16,768,4]{1,2,0:T(4,128)} %bitcast.9) | data formatting | bytes 393216 | tf_op jit(solution)/shard_map/transpose | solution.py:467
  2.2 1.1 %copy.28.cum_ref = f32[16,1,3072]{2,1,0:T(1,128)} copy(f32[16,1,3072]{0,2,1:T(8,128)S(1)} %bitcast.8) | data formatting | bytes 393216 | tf_op jit(solution)/shard_map/reshape | solution.py:467
  3.3 0.0 copy-start.1
  3.3 0.0 copy-start.2
  3.3 19.5 %attention.1 = (bf16[16,2048]{1,0:T(8,128)(2,1)}, bf16[16,4,128]{2,1,0:T(4,128)(2,1)}, f32[16,4]{1,0:T(8,128)}) custom-call(s32[16]{0:T(128)} %lengths_ref.1, bf16[16,2048]{1,0:T(8,128)(2,1)} %tokens_ref.3, f32[16,1,3072]{2,1,0:T(1,128)} %copy.28.cum_ref, f32[1,2048]{1,0:T(1,128)} %bitcast.11, bf16[4,2048]{1,0:T(4,128)(2,1)} %bitcast.10, f32[1,4]{1,0:T(1,128)} %bitcast.13, ...), custom_call_target="tpu_custom_call" | custom-call | tf_op jit(solution)/shard_map/attention/pallas_call | solution.py:469
  22.8 0.0 copy-done.1
  22.8 0.7 %copy.29.ids_ref = s32[16,6]{1,0:T(8,128)} copy(s32[16,6]{0,1:T(8,128)S(1)} %copy-done.1) | data formatting | bytes 768 | tf_op args[18]
  23.5 0.0 copy-done.2
  23.5 0.7 %copy.30.weight_ref = f32[16,6]{1,0:T(8,128)} copy(f32[16,6]{0,1:T(8,128)S(1)} %copy-done.2) | data formatting | bytes 768 | tf_op args[19]
  24.2 0.0 copy-start
  24.2 34.4 %experts.1 = bf16[16,512]{1,0:T(8,128)(2,1)} custom-call(bf16[16,2048]{1,0:T(8,128)(2,1)} %get-tuple-element.6.partial_ref, bf16[16,2048]{1,0:T(8,128)(2,1)} %tokens_ref.3, f32[1,2048]{1,0:T(1,128)} %bitcast.12, s32[16,6]{1,0:T(8,128)} %copy.29.ids_ref, f32[16,6]{1,0:T(8,128)} %copy.30.weight_ref, bf16[2048,128]{1,0:T(8,128)(2,1)} %sg_hbm.1, ...), custom_call_target="tpu_custom_call" | custom-call | tf_op jit(solution)/shard_map/experts/pallas_call | solution.py:513
  58.5 0.0 copy-done
  58.6 0.7 %copy.31 = f32[16,4]{0,1:T(4,128)} copy(f32[16,4]{1,0:T(8,128)S(1)} %copy-done) | data formatting | bytes 512
  59.2 1.3 %copy.33 = bf16[16,512]{1,0:T(8,128)(2,1)} copy(bf16[16,512]{1,0:T(8,128)(2,1)} %experts.1) | data formatting | bytes 32768
Async XLA Ops:
  3.3 19.5 %copy-start.1 = (s32[16,6]{0,1:T(8,128)S(1)}, s32[16,6]{0,1:T(8,128)}, u32[]{:S(2)}) copy-start(s32[16,6]{0,1:T(8,128)} %param.38) | copy-start | bytes 1156
  3.3 20.2 %copy-start.2 = (f32[16,6]{0,1:T(8,128)S(1)}, f32[16,6]{0,1:T(8,128)}, u32[]{:S(2)}) copy-start(f32[16,6]{0,1:T(8,128)} %param.39) | copy-start | bytes 1156
  24.2 34.4 %copy-start = (f32[16,4]{1,0:T(8,128)S(1)}, f32[16,4]{1,0:T(8,128)}, u32[]{:S(2)}) copy-start(f32[16,4]{1,0:T(8,128)} %get-tuple-element.14) | copy-start | bytes 772

commit v2 on v1

--- a/solution.py
+++ b/solution.py
@@ -102,13 +102,26 @@
     column = lax.broadcasted_iota(jnp.int32, (rows, columns), 1)
     own_head = lax.rem(column, heads) == lax.broadcasted_iota(jnp.int32, (rows, columns), 0)
 
+    spread = lax.broadcasted_iota(jnp.int32, (rows, LANES), 1) // heads
+
     def attend(s):
         kv_copy(s).wait()
         length = lengths_ref[s]
         rows_kv = kv[s]
         q = q_pad[s]
         new = fresh[s]
-        cum = cum_ref[s]
+        narrow = cum_ref[s]
+        narrow = jnp.concatenate([narrow] * (rows // heads), axis=0)
+        cum = jnp.concatenate(
+            [
+                jnp.take_along_axis(
+                    narrow[:, b * LANES : (b + 1) * LANES], spread + p * (LANES // heads), axis=1
+                )
+                for b in range(columns // heads // LANES)
+                for p in range(heads)
+            ],
+            axis=1,
+        )
         scores = lax.dot_general(
             q.astype(BF16), rows_kv, (((1,), (1,)), ((), ())), preferred_element_type=F32
         )
@@ -145,7 +158,7 @@
     gathered = jnp.zeros((seqs, LANES), F32)
     for h in range(heads):
         gathered = jnp.where(lane == h, cum_new[:, h, :], gathered)
-    new_cum_ref[...] = gathered[:, :heads]
+    new_cum_ref[...] = gathered.T[:heads, :]
     w_copies[3].wait()
     partial_ref[...] = jnp.dot(attended, wo[...], preferred_element_type=F32).astype(BF16)
 
@@ -174,9 +187,11 @@
     parts,
     from_core,
     to_y,
-    from_y,
     to_x,
-    from_x,
+    big_send,
+    big_recv,
+    small_send,
+    small_recv,
     to_z,
     from_z,
     w_sem,
@@ -260,10 +275,19 @@
     for copy in ar_copies:
         copy.start()
     pad = blocks.shape[3] - half
-    expert_lane = lax.broadcasted_iota(jnp.int32, (seqs, pad), 1)
-    dense = jnp.zeros((seqs, pad), F32)
-    for k in range(ids_ref.shape[1]):
-        dense += jnp.where(ids_ref[:, k : k + 1] == expert_lane, weight_ref[:, k : k + 1], 0.0)
+    expert_row = lax.broadcasted_iota(jnp.int32, (pad, seqs), 0)
+    dense = jnp.zeros((pad, seqs), F32)
+    for k in range(ids_ref.shape[0]):
+        dense += jnp.where(ids_ref[k : k + 1, :] == expert_row, weight_ref[k : k + 1, :], 0.0)
+    unit = lax.broadcasted_iota(jnp.int32, (seqs, seqs), 0) == lax.broadcasted_iota(
+        jnp.int32, (seqs, seqs), 1
+    )
+    dense = lax.dot_general(
+        jnp.where(unit, 1.0, 0.0).astype(BF16),
+        dense.astype(BF16),
+        (((1,), (1,)), ((), ())),
+        preferred_element_type=F32,
+    )
     total = partial_ref[...].astype(F32)
     for k, copy in enumerate(ar_copies):
         copy.wait()
@@ -385,22 +409,35 @@
     own_part(1, y)
     for copy in core_copies:
         copy.wait()
-    parts[0] = (to_y[...] + from_core[1 - y].astype(F32)).astype(BF16)
-    y_copy = remote(parts.at[0], from_y, yx_send.at[0], yx_recv.at[0], (e, y_peer))
-    y_copy.start()
-    to_x[...] = to_x[...] + from_core[y].astype(F32)
-    y_copy.wait()
     half_rows = nz * seqs
+    cut = quarter // 2
     there = pl.ds(pl.multiple_of((1 - x) * half_rows, seqs), half_rows)
     here = pl.ds(pl.multiple_of(x * half_rows, seqs), half_rows)
-    parts[1, :half_rows, :] = (to_x[there, :] + from_y[there, :].astype(F32)).astype(BF16)
-    x_out = remote(
-        parts.at[1, pl.ds(0, half_rows)], from_x, yx_send.at[1], yx_recv.at[1], (x_peer, t)
-    )
-    x_out.start()
-    to_y[:half_rows, :] = to_x[here, :] + from_y[here, :].astype(F32)
-    x_out.wait()
-    to_y[:half_rows, :] = to_y[:half_rows, :] + from_x[...].astype(F32)
+
+    def exchange(src, dst, k, peer):
+        copy = remote(src, dst, yx_send.at[k], yx_recv.at[k], peer)
+        copy.start()
+        return copy
+
+    to_y[...] = to_y[...] + from_core[1 - y].astype(F32)
+    big_send[0] = to_y[:, :cut].astype(BF16)
+    first_y = exchange(big_send.at[0], big_recv.at[0], 0, (e, y_peer))
+    to_x[...] = to_x[...] + from_core[y].astype(F32)
+    big_send[1, :half_rows, :] = to_y[there, cut:].astype(BF16)
+    big_send[1, half_rows:, :] = to_x[there, cut:].astype(BF16)
+    first_x = exchange(big_send.at[1], big_recv.at[1], 1, (x_peer, t))
+    first_y.wait()
+    to_x[:, :cut] = to_x[:, :cut] + big_recv[0].astype(F32)
+    small_send[0] = to_x[there, :cut].astype(BF16)
+    second_x = exchange(small_send.at[0], small_recv.at[0], 2, (x_peer, t))
+    first_x.wait()
+    small_send[1] = (to_y[here, cut:] + big_recv[1, :half_rows, :].astype(F32)).astype(BF16)
+    second_y = exchange(small_send.at[1], small_recv.at[1], 3, (e, y_peer))
+    right = to_x[here, cut:] + big_recv[1, half_rows:, :].astype(F32)
+    second_x.wait()
+    to_y[:half_rows, :cut] = to_x[here, :cut] + small_recv[0].astype(F32)
+    second_y.wait()
+    to_y[:half_rows, cut:] = right + small_recv[1].astype(F32)
     to_z[...] = to_y[:half_rows, :].astype(BF16)
     rz_copies = []
     for d in range(1, nz):
@@ -464,14 +501,13 @@
     smem = pl.BlockSpec(memory_space=pltpu.SMEM)
     anywhere = pl.BlockSpec(memory_space=pl.ANY)
     kv_rows = cache_kv.reshape(seqs, columns, 2 * HEAD_DIM)
-    cum_rows = cache_cum.transpose(0, 2, 1).reshape(seqs, 1, columns)
     per_head = pltpu.VMEM((seqs, head_rows, LANES), F32)
     partial, new_kv, cum_new = pl.pallas_call(
         functools.partial(attention_kernel, 4),
         out_shape=(
             jax.ShapeDtypeStruct((seqs, width), BF16),
             jax.ShapeDtypeStruct((seqs, heads, 2 * HEAD_DIM), BF16),
-            jax.ShapeDtypeStruct((seqs, heads), F32),
+            jax.ShapeDtypeStruct((heads, seqs), F32),
         ),
         in_specs=[smem] + [vmem] * 5 + [anywhere] * 5,
         out_specs=(vmem, vmem, vmem),
@@ -494,7 +530,7 @@
     )(
         lengths,
         tokens,
-        cum_rows,
+        cache_cum,
         norm_attn.reshape(1, width),
         w_forget.T,
         b_forget.reshape(1, heads),
@@ -525,9 +561,11 @@
             pltpu.VMEM((2, token_count, quarter), BF16),
             pltpu.VMEM((2, token_count, quarter), BF16),
             pltpu.VMEM((token_count, quarter), F32),
-            pltpu.VMEM((token_count, quarter), BF16),
             pltpu.VMEM((token_count, quarter), F32),
-            pltpu.VMEM((nz * seqs, quarter), BF16),
+            pltpu.VMEM((2, token_count, quarter // 2), BF16),
+            pltpu.VMEM((2, token_count, quarter // 2), BF16),
+            pltpu.VMEM((2, nz * seqs, quarter // 2), BF16),
+            pltpu.VMEM((2, nz * seqs, quarter // 2), BF16),
             pltpu.VMEM((nz * seqs, quarter), BF16),
             pltpu.VMEM((nz - 1, seqs, quarter), BF16),
             dma((3 * experts + 3,)),
@@ -539,8 +577,8 @@
             dma((ep_size,)),
             dma((2,)),
             dma((2,)),
-            dma((2,)),
-            dma((2,)),
+            dma((4,)),
+            dma((4,)),
             dma((nz - 1,)),
             dma((nz - 1,)),
         ],
@@ -552,8 +590,8 @@
         partial,
         tokens,
         norm_ffn.reshape(1, width),
-        route_ids,
-        route_weight,
+        route_ids.T,
+        route_weight.T,
         shared_gate,
         shared_up,
         shared_down,
@@ -561,7 +599,7 @@
         expert_up,
         expert_down,
     )
-    return (output, new_kv, cum_new)
+    return (output, new_kv, cum_new.T)
 
 
 def shards_general(

time: 60.8 us -> 55.4 us (0.911)
  local copies, waits for them, and re-layouts: 6.01 us -> 1.32 us
  Pallas kernels: 53.9 us -> 53.2 us
    unnamed x10 -> x1, local copies, waits for them, and re-layouts: 3.34 us -> 1.32 us
    transpose x1 -> x0, local copies, waits for them, and re-layouts: 1.55 us -> none  [shards(): cum_rows = cache_cum.transpose(0, 2, 1).reshape(seqs, 1, columns)]
    reshape x1 -> x0, local copies, waits for them, and re-layouts: 1.11 us -> none  [shards(): cum_rows = cache_cum.transpose(0, 2, 1).reshape(seqs, 1, columns)]
    pallas_call x1, Pallas kernels: 34.4 us -> 33.7 us  [shards(): pl.pallas_call(functools.partial(expert_kernel, ep_size, tp_size), out_sh...]
where the time goes in v2:
time: 55.4 us; the launch traced here: 55.1 us
  Pallas kernels  53.2 us (96%)
  local copies, waits for them, and re-layouts  1.32 us (2%)
  between operations  0.65 us (1%)
    pallas_call x1, Pallas kernels, shards(): pl.pallas_call(functools.partial(expert_kernel, ep_size, tp_size), out_sh...  33.7 us
    pallas_call x1, Pallas kernels, shards(): pl.pallas_call(functools.partial(attention_kernel, 4), out_shape=(jax.Sha...  19.4 us
    unnamed x1, local copies, waits for them, and re-layouts  1.32 us

profile of v2, /device:TPU:0, one launch (start us, length us, event | category | flops | bytes accessed | tf_op | source)
XLA Modules:
  0.0 55.1 jit_solution(14960682650862227293)
XLA Ops:
  0.6 19.4 %attention.1 = (bf16[16,2048]{1,0:T(8,128)(2,1)}, bf16[16,4,128]{2,1,0:T(4,128)(2,1)}, f32[4,16]{1,0:T(4,128)}) custom-call(s32[16]{0:T(128)} %lengths_ref.1, bf16[16,2048]{1,0:T(8,128)(2,1)} %tokens_ref.3, f32[16,4,768]{2,1,0:T(4,128)} %cum_ref.1, f32[1,2048]{1,0:T(1,128)} %bitcast.10, bf16[4,2048]{1,0:T(4,128)(2,1)} %bitcast.9, f32[1,4]{1,0:T(1,128)} %bitcast.14, ...), custom_call_target="tpu_custom_call" | custom-call | tf_op jit(solution)/shard_map/attention/pallas_call | solution.py:505
  20.1 33.7 %experts.1 = bf16[16,512]{1,0:T(8,128)(2,1)} custom-call(bf16[16,2048]{1,0:T(8,128)(2,1)} %get-tuple-element.6.partial_ref, bf16[16,2048]{1,0:T(8,128)(2,1)} %tokens_ref.3, f32[1,2048]{1,0:T(1,128)} %bitcast.11, s32[6,16]{1,0:T(8,128)} %bitcast.12, f32[6,16]{1,0:T(8,128)} %bitcast.13, bf16[2048,128]{1,0:T(8,128)(2,1)} %sg_hbm.1, bf16[2048,128]{1,0:T(8,128)(2,1)} %su_hbm.1, ...), custom_call_target="tpu_custom_call" | custom-call | tf_op jit(solution)/shard_map/experts/pallas_call | solution.py:549
  53.8 1.3 %copy.24 = bf16[16,512]{1,0:T(8,128)(2,1)} copy(bf16[16,512]{1,0:T(8,128)(2,1)} %experts.1) | data formatting | bytes 32768
